TPU v7x, 512 devices: a whole 4x8x8 slice. The times are simulated.
512 devices in a mesh: ep: 128 (over z, y, core), tp: 4 (over x).
Axes of the slice: x: 4, y: 8, z: 8, core: 2. Of those that a mesh axis runs over, the one named last changes fastest.
Arguments:
- tokens: bfloat16 [2048, 1024], P('ep'), may hold values from -24 to 24
- seq_length: int32 [2048], P('ep'), may hold values from 1024 to 16383
- ret_state: float32 [2048, 4, 128, 256], P('ep', 'tp'), may hold values from -0.6 to 0.6
- norm_in: float32 [1024], replicated, may hold values from 0.1 to 1.9
- w_query: bfloat16 [1024, 512], P(None, 'tp'), may hold values from -0.1875 to 0.1875
- w_key: bfloat16 [1024, 512], P(None, 'tp'), may hold values from -0.1875 to 0.1875
- w_value: bfloat16 [1024, 1024], P(None, 'tp'), may hold values from -0.1875 to 0.1875
- head_gain: float32 [1024], P('tp'), may hold values from 0.1 to 1.9
- w_output: bfloat16 [1024, 1024], P('tp'), may hold values from -0.1875 to 0.1875
- norm_mid: float32 [1024], replicated, may hold values from 0.1 to 1.9
- route_expert: int32 [2048, 2], P('ep'), may hold values from 0 to 63, all different within a row; in each aligned block of 16 rows (0 to 15, 16 to 31, ...) at most 2 rows name the same one
- route_score: float32 [2048, 2], P('ep'), may hold values from -6 to 6
- expert_gate: bfloat16 [128, 1024, 1792], P('ep', None, 'tp'), may hold values from -0.1875 to 0.1875
- expert_up: bfloat16 [128, 1024, 1792], P('ep', None, 'tp'), may hold values from -0.1875 to 0.1875
- expert_down: bfloat16 [128, 1792, 1024], P('ep', 'tp'), may hold values from -0.09375 to 0.09375
Outputs:
- mixed: bfloat16 [2048, 1024], P('ep', 'tp')
Inputs may be any that keep to these rules, and one draw needn't show every extreme that they name: `route_expert`: each row names 2 different experts; within the rows of one device no expert is named by more than 2 rows, and some device's rows name one expert exactly 2 times.
All inputs are finite; a program needn't handle non-finite values.
Results may differ from a plain program's by a relative error of at most 0.014.
Values may be sent and summed in bfloat16 or wider, within the bound.
A program may use at most 64 MiB of HBM per device.

v0:
```python
import jax
import jax.numpy as jnp
from jax import lax
from jax.sharding import PartitionSpec as P

DK = 128
DV = 256
SPREAD = 2
TOP_K = 2
EPS = 1e-06


def in_blocks(x, dim, devices):
    lengths = x.shape
    pieces = x.reshape(*lengths[:dim], devices, lengths[dim] // devices, *lengths[dim + 1 :])
    return jnp.moveaxis(pieces, dim, 0)


def summed_on_arrival(x, axis, dim):
    pieces = in_blocks(x, dim, lax.axis_size(axis))
    arrived = lax.all_to_all(pieces, axis, split_axis=0, concat_axis=0, tiled=True)
    return arrived.astype(jnp.float32).sum(axis=0)


def copy_for_each(x, axis):
    copies = jnp.broadcast_to(x, (lax.axis_size(axis), *x.shape))
    return lax.all_to_all(copies, axis, split_axis=0, concat_axis=0, tiled=True)


def over_copies(x, axis):
    return copy_for_each(x, axis).astype(jnp.float32).sum(axis=0)


def rotate(head_rows, positions):
    half_width = head_rows.shape[-1] // 2
    inverse = 10000.0 ** (-jnp.arange(half_width, dtype=jnp.float32) / half_width)
    angles = positions[:, None] * inverse[None, :]
    cosine = jnp.cos(angles)[:, None, :]
    sine_part = jnp.sin(angles)[:, None, :]
    first_half = head_rows[..., :half_width]
    second = head_rows[..., half_width:]
    return jnp.concatenate(
        [first_half * cosine - second * sine_part, first_half * sine_part + second * cosine],
        axis=-1,
    )


def body(
    tokens,
    seq_length,
    ret_state,
    norm_in,
    w_query,
    w_key,
    w_value,
    head_gain,
    w_output,
    norm_mid,
    route_expert,
    route_score,
    expert_gate,
    expert_up,
    expert_down,
):
    n_lanes = lax.axis_size("tp")
    n_groups = lax.axis_size("ep")
    lane_index = lax.axis_index("tp")
    local_rows = tokens.shape[0]
    width = tokens.shape[1]
    quarter = width // n_lanes
    heads_here = w_query.shape[1] // DK
    token_f = tokens.astype(jnp.float32)
    normed = (
        token_f * lax.rsqrt(jnp.mean(token_f * token_f, axis=-1, keepdims=True) + EPS) * norm_in
    ).astype(jnp.bfloat16)
    query_proj = jnp.dot(normed, w_query, preferred_element_type=jnp.float32).astype(jnp.bfloat16)
    key_proj = jnp.dot(normed, w_key, preferred_element_type=jnp.float32).astype(jnp.bfloat16)
    value_proj = jnp.dot(normed, w_value, preferred_element_type=jnp.float32).astype(jnp.bfloat16)
    positions = seq_length.astype(jnp.float32)
    q_rot = rotate(query_proj.astype(jnp.float32).reshape(local_rows, heads_here, DK), positions)
    k_rot = rotate(
        key_proj.astype(jnp.float32).reshape(local_rows, heads_here, DK), positions
    ) * DK ** (-0.5)
    value_rows = value_proj.astype(jnp.float32).reshape(local_rows, heads_here, DV)
    head_index = (lane_index * heads_here + jnp.arange(heads_here, dtype=jnp.int32)).astype(
        jnp.float32
    )
    decay_rate = 1.0 - jnp.exp2(-2.0 - 2.0 * head_index)
    carried = jnp.einsum("bhd,bhde->bhe", q_rot, ret_state)
    within = jnp.sum(q_rot * k_rot, axis=-1, keepdims=True) * value_rows
    retained = decay_rate[None, :, None] * carried + within
    centre = jnp.mean(retained, axis=-1, keepdims=True)
    variance = jnp.mean(jnp.square(retained - centre), axis=-1, keepdims=True)
    ret_out = ((retained - centre) * lax.rsqrt(variance + EPS)).reshape(local_rows, heads_here * DV)
    ret_out = (ret_out * head_gain).astype(jnp.bfloat16)
    partial_value = jnp.dot(ret_out, w_output, preferred_element_type=jnp.float32)
    experts_n = n_groups // SPREAD
    cap = min(local_rows, max(2, 3 * local_rows * TOP_K // (2 * experts_n)))
    flat_rows = route_expert.reshape(-1)
    onehot = (flat_rows[:, None] == jnp.arange(experts_n, dtype=jnp.int32)[None, :]).astype(
        jnp.int32
    )
    rank_index = jnp.sum((jnp.cumsum(onehot, axis=0) - onehot) * onehot, axis=1)
    slot_index = flat_rows * cap + rank_index
    chosen_slot = (
        slot_index[:, None] == jnp.arange(experts_n * cap, dtype=jnp.int32)[None, :]
    ).astype(jnp.float32)
    chosen_slot = chosen_slot.reshape(local_rows, TOP_K, experts_n * cap)
    placing = jnp.sum(chosen_slot, axis=1).astype(jnp.bfloat16)
    weights = jax.nn.softmax(route_score, axis=-1)
    combine = jnp.sum(chosen_slot * weights[:, :, None], axis=1)
    gate_rows = expert_gate[0]
    up_rows = expert_up[0]
    down_rows = expert_down[0]
    attended = over_copies(partial_value.astype(jnp.bfloat16), "tp").astype(jnp.float32)
    resid_full = (token_f + attended).astype(jnp.bfloat16)
    resid_f = resid_full.astype(jnp.float32)
    mid_full = (
        resid_f * lax.rsqrt(jnp.mean(resid_f * resid_f, axis=-1, keepdims=True) + EPS) * norm_mid
    ).astype(jnp.bfloat16)
    resid = lax.dynamic_slice_in_dim(resid_full, lane_index * quarter, quarter, 1)
    mid = lax.dynamic_slice_in_dim(mid_full, lane_index * quarter, quarter, 1)
    packed = jnp.einsum("re,rc->ec", placing, mid, preferred_element_type=jnp.float32).astype(
        jnp.bfloat16
    )
    packed = packed.reshape(experts_n, cap, quarter)
    send_buffer = jnp.repeat(packed, SPREAD, axis=0)
    received = lax.all_to_all(send_buffer, "ep", split_axis=0, concat_axis=0, tiled=True)
    groups, row_count, cols = received.shape
    piece_cols = lax.all_gather(received, "tp", axis=2, tiled=True)
    piece_width = piece_cols.shape[2]
    flat_in = piece_cols.reshape(groups * row_count, piece_width)
    gate_sum = jnp.dot(flat_in, gate_rows, preferred_element_type=jnp.float32)
    up_sum = jnp.dot(flat_in, up_rows, preferred_element_type=jnp.float32)
    hidden = (jax.nn.silu(gate_sum) * up_sum).astype(jnp.bfloat16)
    down_part = jnp.dot(hidden, down_rows, preferred_element_type=jnp.float32)
    share = summed_on_arrival(down_part.astype(jnp.bfloat16), "tp", 1)
    returned = share.astype(jnp.bfloat16).reshape(groups, row_count, share.shape[1])
    arrived = lax.all_to_all(returned, "ep", split_axis=0, concat_axis=0, tiled=True)
    part_total = jnp.sum(
        arrived.reshape(experts_n, SPREAD, cap, quarter).astype(jnp.float32), axis=1
    )
    expert_out = part_total.astype(jnp.bfloat16)
    expert_mix = jnp.dot(combine, expert_out.reshape(experts_n * cap, quarter).astype(jnp.float32))
    return (resid.astype(jnp.float32) + expert_mix).astype(jnp.bfloat16)


def solution(mesh):
    placed = (
        P("ep", None),
        P("ep"),
        P("ep", "tp", None, None),
        P(),
        P(None, "tp"),
        P(None, "tp"),
        P(None, "tp"),
        P("tp"),
        P("tp", None),
        P(),
        P("ep", None),
        P("ep", None),
        P("ep", None, "tp"),
        P("ep", None, "tp"),
        P("ep", "tp", None),
    )
    return jax.shard_map(body, mesh=mesh, in_specs=placed, out_specs=P("ep", "tp"), check_vma=False)
```

profile of v0, /device:TPU:1, one launch (start us, length us, event | category | flops | bytes accessed | tf_op | source)
XLA Modules:
  0.0 94.6 jit_solution(541615782359818185)
XLA Ops:
  0.0 0.0 copy-start
  0.0 0.0 copy-start.6
  0.0 0.0 copy-start.1
  0.0 0.0 copy-start.5
  0.1 0.8 convert_element_type.79
  0.9 1.0 %fusion.22 = f32[16]{0:T(128)S(1)} fusion(bf16[16,1024]{1,0:T(8,128)(2,1)} %param.15), kind=kLoop, calls=%fused_computation.35 | loop fusion | flops 49136 | bytes 32832 | tf_op jit(solution)/shard_map/reduce_sum | solution.py:74
  1.9 1.2 %fusion.10 = f32[16,1,128]{2,0,1:T(8,128)S(1)} fusion(bf16[1024,128]{1,0:T(8,128)(2,1)} %param.20, bf16[16,1024]{1,0:T(8,128)(2,1)} %param.15, f32[1024]{0:T(1024)} %param.18, f32[16]{0:T(128)S(1)} %add_rsqrt_fusion.2), kind=kOutput, calls=%fused_computation.18 | convolution fusion | flops 4263936 | bytes 307264 | tf_op jit(solution)/shard_map/dot_general | solution.py:77
  3.1 0.0 copy-start.4
  3.1 1.2 %fusion.8 = f32[16,1,128]{2,0,1:T(8,128)S(1)} fusion(bf16[1024,128]{1,0:T(8,128)(2,1)} %param.19, bf16[16,1024]{1,0:T(8,128)(2,1)} %param.15, f32[1024]{0:T(1024)} %param.18, f32[16]{0:T(128)S(1)} %add_rsqrt_fusion.2), kind=kOutput, calls=%fused_computation.16 | convolution fusion | flops 4263936 | bytes 307264 | tf_op jit(solution)/shard_map/dot_general | solution.py:76
  4.3 0.1 fusion.37
  4.5 0.2 fusion.45
  4.6 0.0 copy-done
  4.6 0.3 fusion.60
  4.9 0.0 copy-done.2
  4.9 0.0 copy-done.7
  4.9 0.0 copy-done.6
  4.9 0.3 fusion.59
  5.3 0.2 multiply_reduce_fusion.1
  5.5 0.0 copy-done.1
  5.5 0.0 copy-done.5
  5.5 0.2 convolution_convert_fusion.2
  5.7 0.7 broadcast_in_dim.4
  6.4 4.8 %all-to-all-start = ((bf16[4,16,1024]{2,1,0:T(8,128)(2,1)}), bf16[4,16,1024]{2,1,0:T(8,128)(2,1)S(1)}, u32[]{:S(2)}, u32[]{:S(2)}) async-start(bf16[4,16,1024]{2,1,0:T(8,128)(2,1)} %broadcast_in_dim.4), calls=%async_computation | async-start | bytes 262144 | tf_op jit(solution)/shard_map/all_to_all | solution.py:27
  11.2 0.0 copy-done.3
  11.2 0.1 copy.41
  11.3 0.1 eq.29
  11.4 0.1 fusion.28
  11.5 0.1 reduce_window_sum.11
  11.6 0.2 select_reduce_fusion.1
  11.7 0.1 reduce_sum.122
  11.8 0.1 copy.42
  11.9 0.8 dynamic-slice
  12.7 0.1 convert_reduce_fusion.1
  12.8 3.2 %all-to-all-done = bf16[4,16,1024]{2,1,0:T(8,128)(2,1)S(1)} async-done(((bf16[4,16,1024]{2,1,0:T(8,128)(2,1)}), bf16[4,16,1024]{2,1,0:T(8,128)(2,1)S(1)}, u32[]{:S(2)}, u32[]{:S(2)}) %all-to-all-start) | async-done | bytes 131104 | tf_op jit(solution)/shard_map/all_to_all | solution.py:27
  16.0 0.1 multiply_reduce_fusion
  16.2 0.2 convolution_convert_fusion.1
  16.4 0.1 broadcast_in_dim.5
  16.5 31.5 %all_to_all.20 = bf16[128,2,256]{2,1,0:T(2,128)(2,1)S(1)} all-to-all(bf16[128,2,256]{2,1,0:T(2,128)(2,1)S(1)} %bitcast.62), channel_id=1, replica_groups=mesh['ep'=128,'tp'=4] {'ep'}, dimensions={0} | all-to-all | bytes 262144 | tf_op jit(solution)/shard_map/all_to_all | solution.py:128
  48.0 9.7 %all_gather.3 = bf16[128,2,1024]{2,1,0:T(2,128)(2,1)S(1)} all-gather(bf16[128,2,256]{2,1,0:T(2,128)(2,1)S(1)} %all_to_all.20), channel_id=1, replica_groups=mesh['ep'=128,'tp'=4] {'tp'}, dimensions={2}, use_global_device_ids=true | all-gather | bytes 655360 | tf_op jit(solution)/shard_map/all_gather | solution.py:130
  57.8 0.2 reshape.276
  58.0 2.4 %fusion.14 = f32[256,448]{0,1:T(8,128)} fusion(bf16[256,1024]{1,0:T(8,128)(2,1)S(1)} %reshape.276, bf16[1,1024,448]{1,2,0:T(8,128)(2,1)} %param.27), kind=kOutput, calls=%fused_computation.21 | convolution fusion | flops 234881024 | bytes 1900544 | tf_op jit(solution)/shard_map/dot_general | solution.py:133
  60.4 2.9 %convolution_convert_fusion = bf16[256,1024]{1,0:T(8,128)(2,1)S(1)} fusion(bf16[256,1024]{1,0:T(8,128)(2,1)S(1)} %reshape.276, bf16[1,448,1024]{2,1,0:T(8,128)(2,1)} %param.29, bf16[1,1024,448]{1,2,0:T(8,128)(2,1)} %param.28, f32[256,448]{0,1:T(8,128)} %fusion.14), kind=kOutput, calls=%fused_computation.2 | convolution fusion | flops 470712320 | bytes 3342336 | tf_op jit(solution)/shard_map/dot_general | solution.py:136
  63.3 9.6 %all_to_all.21 = bf16[4,256,256]{2,1,0:T(8,128)(2,1)S(1)} all-to-all(bf16[4,256,256]{2,1,0:T(8,128)(2,1)S(1)} %bitcast.60), channel_id=1, replica_groups=mesh['ep'=128,'tp'=4] {'tp'}, dimensions={0} | all-to-all | bytes 1048576 | tf_op jit(solution)/shard_map/all_to_all | solution.py:21
  72.9 0.1 reduce_sum.127
  73.0 0.1 reshape.278
  73.0 20.6 %all_to_all.22 = bf16[128,2,256]{2,1,0:T(2,128)(2,1)S(1)} all-to-all(bf16[128,2,256]{2,1,0:T(2,128)(2,1)S(1)} %reshape.278), channel_id=1, replica_groups=mesh['ep'=128,'tp'=4] {'ep'}, dimensions={0} | all-to-all | bytes 262144 | tf_op jit(solution)/shard_map/all_to_all | solution.py:139
  93.7 0.2 bitcast_reduce_fusion
  93.9 0.7 fusion.3
  (18 shorter events, 0.2 us)
Async XLA Ops:
  0.0 4.6 %copy-start = (f32[16,1,128,256]{3,2,1,0:T(8,128)S(1)}, f32[16,1,128,256]{3,2,1,0:T(8,128)}, u32[]{:S(2)}) copy-start(f32[16,1,128,256]{3,2,1,0:T(8,128)} %param.17) | copy-start | bytes 6291460
  0.0 4.9 %copy-start.2 = (bf16[16,1024]{1,0:T(8,128)(2,1)S(1)}, bf16[16,1024]{1,0:T(8,128)(2,1)}, u32[]{:S(2)}) copy-start(bf16[16,1024]{1,0:T(8,128)(2,1)} %param.15) | copy-start | bytes 98308
  0.0 4.9 %copy-start.7 = (f32[1024]{0:T(1024)S(1)}, f32[1024]{0:T(1024)}, u32[]{:S(2)}) copy-start(f32[1024]{0:T(1024)} %param.18) | copy-start | bytes 12292
  0.0 4.9 %copy-start.6 = (bf16[1024,256]{1,0:T(8,128)(2,1)S(1)}, bf16[1024,256]{1,0:T(8,128)(2,1)}, u32[]{:S(2)}) copy-start(bf16[1024,256]{1,0:T(8,128)(2,1)} %param.21) | copy-start | bytes 1572868
  0.0 5.4 %copy-start.1 = (bf16[256,1024]{1,0:T(8,128)(2,1)S(1)}, bf16[256,1024]{1,0:T(8,128)(2,1)}, u32[]{:S(2)}) copy-start(bf16[256,1024]{1,0:T(8,128)(2,1)} %param.23) | copy-start | bytes 1572868
  0.0 5.4 %copy-start.5 = (f32[256]{0:T(256)S(1)}, f32[256]{0:T(256)}, u32[]{:S(2)}) copy-start(f32[256]{0:T(256)} %param.22) | copy-start | bytes 3076
  3.1 8.1 %copy-start.3 = (f32[16,2]{0,1:T(2,128)S(1)}, f32[16,2]{0,1:T(2,128)}, u32[]{:S(2)}) copy-start(f32[16,2]{0,1:T(2,128)} %param.26) | copy-start | bytes 388
  3.1 8.2 %copy-start.4 = (s32[16,2]{0,1:T(2,128)S(1)}, s32[16,2]{0,1:T(2,128)}, u32[]{:S(2)}) copy-start(s32[16,2]{0,1:T(2,128)} %param.25) | copy-start | bytes 388
  6.4 9.7 %all-to-all-start = ((bf16[4,16,1024]{2,1,0:T(8,128)(2,1)}), bf16[4,16,1024]{2,1,0:T(8,128)(2,1)S(1)}, u32[]{:S(2)}, u32[]{:S(2)}) async-start(bf16[4,16,1024]{2,1,0:T(8,128)(2,1)} %broadcast_in_dim.4), calls=%async_computation | async-start | bytes 262144 | tf_op jit(solution)/shard_map/all_to_all | solution.py:27
where the time goes:
time: 95 us; the launch traced here: 94.6 us
  blocking collectives  71.5 us (75%)
  matrix products  9.44 us (10%)
  starting transfers between devices  4.83 us (5%)
  waiting for transfers between devices  3.24 us (3%)
  other arithmetic  3.14 us (3%)
  local copies, waits for them, and re-layouts  2.24 us (2%)
    all_to_all x1, blocking collectives, body(): lax.all_to_all(send_buffer, 'ep', split_axis=0, concat_axis=0, tiled=True)  31.5 us
    all_to_all x1, blocking collectives, body(): lax.all_to_all(returned, 'ep', split_axis=0, concat_axis=0, tiled=True)  20.6 us
    all_gather x1, blocking collectives, body(): piece_cols = lax.all_gather(received, 'tp', axis=2, tiled=True)  9.74 us
    all_to_all x1, blocking collectives, summed_on_arrival(): lax.all_to_all(pieces, axis, split_axis=0, concat_axis=0, tiled=True)  9.56 us
    all_to_all x1, starting transfers between devices, copy_for_each(): return lax.all_to_all(copies, axis, split_axis=0, concat_axis=0, tiled=True)  4.83 us
    all_to_all x1, waiting for transfers between devices, copy_for_each(): return lax.all_to_all(copies, axis, split_axis=0, concat_axis=0, tiled=True)  3.24 us
    dot_general x1, matrix products, body(): down_part = jnp.dot(hidden, down_rows, preferred_element_type=jnp.float32)  2.9 us
    dot_general x1, matrix products, body(): gate_sum = jnp.dot(flat_in, gate_rows, preferred_element_type=jnp.float32)  2.4 us
  transfers between devices with their start and end apart: 1, of which 1 were waited for; matrix products, arithmetic and copies ran while one was open for 2% of the time, Pallas kernels for 0%

commit v1 on v0

--- a/solution.py
+++ b/solution.py
@@ -127,7 +127,9 @@
     send_buffer = jnp.repeat(packed, SPREAD, axis=0)
     received = lax.all_to_all(send_buffer, "ep", split_axis=0, concat_axis=0, tiled=True)
     groups, row_count, cols = received.shape
-    piece_cols = lax.all_gather(received, "tp", axis=2, tiled=True)
+    piece_cols = jnp.concatenate(
+        lax.all_to_all(jnp.stack([received] * lax.axis_size("tp")), "tp", 0, 0), axis=2
+    )
     piece_width = piece_cols.shape[2]
     flat_in = piece_cols.reshape(groups * row_count, piece_width)
     gate_sum = jnp.dot(flat_in, gate_rows, preferred_element_type=jnp.float32)

time: 95 us -> 96.7 us (1.018)
  blocking collectives: 71.5 us -> 73.4 us
  matrix products: 9.44 us -> 8.25 us
    all_to_all x0 -> x1, blocking collectives: none -> 11.6 us  [body(): lax.all_to_all(jnp.stack([received] * lax.axis_size('tp')), 'tp', 0, 0)]
    all_gather x1 -> x0, blocking collectives: 9.74 us -> none  [body(): piece_cols = lax.all_gather(received, 'tp', axis=2, tiled=True)]
    dot_general x1, matrix products: 2.4 us -> 1.21 us  [body(): gate_sum = jnp.dot(flat_in, gate_rows, preferred_element_type=jnp.float32)]
    all_to_all x1, blocking collectives: 9.56 us -> 10.7 us  [summed_on_arrival(): lax.all_to_all(pieces, axis, split_axis=0, concat_axis=0, tiled=True)]
    all_to_all x1, blocking collectives: 20.6 us -> 19.5 us  [body(): lax.all_to_all(returned, 'ep', split_axis=0, concat_axis=0, tiled=True)]
where the time goes in v1:
time: 96.7 us; the launch traced here: 96.3 us
  blocking collectives  73.4 us (76%)
  matrix products  8.25 us (9%)
  starting transfers between devices  4.83 us (5%)
  waiting for transfers between devices  3.24 us (3%)
  other arithmetic  3.14 us (3%)
  local copies, waits for them, and re-layouts  3.1 us (3%)
    all_to_all x1, blocking collectives, body(): lax.all_to_all(send_buffer, 'ep', split_axis=0, concat_axis=0, tiled=True)  31.7 us
    all_to_all x1, blocking collectives, body(): lax.all_to_all(returned, 'ep', split_axis=0, concat_axis=0, tiled=True)  19.5 us
    all_to_all x1, blocking collectives, body(): lax.all_to_all(jnp.stack([received] * lax.axis_size('tp')), 'tp', 0, 0)  11.6 us
    all_to_all x1, blocking collectives, summed_on_arrival(): lax.all_to_all(pieces, axis, split_axis=0, concat_axis=0, tiled=True)  10.7 us
    all_to_all x1, starting transfers between devices, copy_for_each(): return lax.all_to_all(copies, axis, split_axis=0, concat_axis=0, tiled=True)  4.83 us
    all_to_all x1, waiting for transfers between devices, copy_for_each(): return lax.all_to_all(copies, axis, split_axis=0, concat_axis=0, tiled=True)  3.24 us
    dot_general x1, matrix products, body(): down_part = jnp.dot(hidden, down_rows, preferred_element_type=jnp.float32)  2.9 us
  transfers between devices with their start and end apart: 1, of which 1 were waited for; matrix products, arithmetic and copies ran while one was open for 2% of the time, Pallas kernels for 0%

profile of v1, /device:TPU:1, one launch (start us, length us, event | category | flops | bytes accessed | tf_op | source)
XLA Modules:
  0.0 96.3 jit_solution(12211598417894578315)
XLA Ops:
  0.0 0.0 copy-start
  0.0 0.0 copy-start.7
  0.0 0.0 copy-start.2
  0.0 0.0 copy-start.6
  0.1 0.8 convert_element_type.79
  0.9 1.0 %fusion.22 = f32[16]{0:T(128)S(1)} fusion(bf16[16,1024]{1,0:T(8,128)(2,1)} %param.15), kind=kLoop, calls=%fused_computation.35 | loop fusion | flops 49136 | bytes 32832 | tf_op jit(solution)/shard_map/reduce_sum | solution.py:74
  1.9 1.2 %fusion.10 = f32[16,1,128]{2,0,1:T(8,128)S(1)} fusion(bf16[1024,128]{1,0:T(8,128)(2,1)} %param.20, bf16[16,1024]{1,0:T(8,128)(2,1)} %param.15, f32[1024]{0:T(1024)} %param.18, f32[16]{0:T(128)S(1)} %add_rsqrt_fusion.2), kind=kOutput, calls=%fused_computation.18 | convolution fusion | flops 4263936 | bytes 307264 | tf_op jit(solution)/shard_map/dot_general | solution.py:77
  3.1 0.0 copy-start.5
  3.1 1.2 %fusion.8 = f32[16,1,128]{2,0,1:T(8,128)S(1)} fusion(bf16[1024,128]{1,0:T(8,128)(2,1)} %param.19, bf16[16,1024]{1,0:T(8,128)(2,1)} %param.15, f32[1024]{0:T(1024)} %param.18, f32[16]{0:T(128)S(1)} %add_rsqrt_fusion.2), kind=kOutput, calls=%fused_computation.16 | convolution fusion | flops 4263936 | bytes 307264 | tf_op jit(solution)/shard_map/dot_general | solution.py:76
  4.3 0.1 fusion.37
  4.5 0.2 fusion.45
  4.6 0.0 copy-done
  4.6 0.3 fusion.60
  4.9 0.0 copy-done.3
  4.9 0.0 copy-done.8
  4.9 0.0 copy-done.7
  4.9 0.3 fusion.59
  5.3 0.2 multiply_reduce_fusion.1
  5.5 0.2 convolution_convert_fusion.2
  5.7 0.7 broadcast_in_dim.4
  6.4 4.8 %all-to-all-start = ((bf16[4,16,1024]{2,1,0:T(8,128)(2,1)}), bf16[4,16,1024]{2,1,0:T(8,128)(2,1)S(1)}, u32[]{:S(2)}, u32[]{:S(2)}) async-start(bf16[4,16,1024]{2,1,0:T(8,128)(2,1)} %broadcast_in_dim.4), calls=%async_computation | async-start | bytes 262144 | tf_op jit(solution)/shard_map/all_to_all | solution.py:27
  11.2 0.1 copy.44
  11.3 0.1 eq.29
  11.4 0.1 fusion.28
  11.5 0.1 reduce_window_sum.11
  11.6 0.2 select_reduce_fusion.1
  11.7 0.1 reduce_sum.122
  11.8 0.1 copy.45
  11.9 0.8 dynamic-slice
  12.7 0.1 convert_reduce_fusion.1
  12.8 3.2 %all-to-all-done = bf16[4,16,1024]{2,1,0:T(8,128)(2,1)S(1)} async-done(((bf16[4,16,1024]{2,1,0:T(8,128)(2,1)}), bf16[4,16,1024]{2,1,0:T(8,128)(2,1)S(1)}, u32[]{:S(2)}, u32[]{:S(2)}) %all-to-all-start) | async-done | bytes 131104 | tf_op jit(solution)/shard_map/all_to_all | solution.py:27
  16.0 0.1 multiply_reduce_fusion
  16.2 0.2 convolution_convert_fusion.1
  16.4 0.0 copy-start.1
  16.4 0.1 broadcast_in_dim.5
  16.5 31.7 %all_to_all.25 = bf16[128,2,256]{2,1,0:T(2,128)(2,1)S(1)} all-to-all(bf16[128,2,256]{2,1,0:T(2,128)(2,1)S(1)} %bitcast.70), channel_id=1, replica_groups=mesh['ep'=128,'tp'=4] {'ep'}, dimensions={0} | all-to-all | bytes 262144 | tf_op jit(solution)/shard_map/all_to_all | solution.py:128
  48.2 0.3 stack.2
  48.5 11.6 %all_to_all.26 = bf16[4,128,2,256]{3,2,1,0:T(2,128)(2,1)S(1)} all-to-all(bf16[4,128,2,256]{3,2,1,0:T(2,128)(2,1)S(1)} %stack.2), channel_id=1, replica_groups=mesh['ep'=128,'tp'=4] {'tp'}, dimensions={0} | all-to-all | bytes 1048576 | tf_op jit(solution)/shard_map/all_to_all | solution.py:131
  60.0 0.7 copy.46
  60.7 0.1 copy.54
  60.8 1.2 %fusion.14 = f32[256,448]{0,1:T(8,128)} fusion(bf16[256,1024]{1,0:T(8,128)(2,1)S(1)} %bitcast.67, bf16[1,1024,448]{1,2,0:T(8,128)(2,1)S(1)} %copy-done.1), kind=kOutput, calls=%fused_computation.21 | convolution fusion | flops 234881024 | bytes 1900544 | tf_op jit(solution)/shard_map/dot_general | solution.py:135
  62.1 2.9 %convolution_convert_fusion = bf16[256,1024]{1,0:T(8,128)(2,1)S(1)} fusion(bf16[256,1024]{1,0:T(8,128)(2,1)S(1)} %bitcast.68, bf16[1,448,1024]{2,1,0:T(8,128)(2,1)} %param.29, bf16[1,1024,448]{1,2,0:T(8,128)(2,1)} %param.28, f32[256,448]{0,1:T(8,128)} %fusion.14), kind=kOutput, calls=%fused_computation.2 | convolution fusion | flops 470712320 | bytes 3342336 | tf_op jit(solution)/shard_map/dot_general | solution.py:138
  65.0 10.7 %all_to_all.27 = bf16[4,256,256]{2,1,0:T(8,128)(2,1)S(1)} all-to-all(bf16[4,256,256]{2,1,0:T(8,128)(2,1)S(1)} %bitcast.66), channel_id=1, replica_groups=mesh['ep'=128,'tp'=4] {'tp'}, dimensions={0} | all-to-all | bytes 1048576 | tf_op jit(solution)/shard_map/all_to_all | solution.py:21
  75.7 0.1 reduce_sum.127
  75.8 0.1 reshape.280
  75.9 19.5 %all_to_all.28 = bf16[128,2,256]{2,1,0:T(2,128)(2,1)S(1)} all-to-all(bf16[128,2,256]{2,1,0:T(2,128)(2,1)S(1)} %reshape.280), channel_id=1, replica_groups=mesh['ep'=128,'tp'=4] {'ep'}, dimensions={0} | all-to-all | bytes 262144 | tf_op jit(solution)/shard_map/all_to_all | solution.py:141
  95.3 0.2 bitcast_reduce_fusion
  95.5 0.7 fusion.3
  (22 shorter events, 0.2 us)
Async XLA Ops:
  0.0 4.6 %copy-start = (f32[16,1,128,256]{3,2,1,0:T(8,128)S(1)}, f32[16,1,128,256]{3,2,1,0:T(8,128)}, u32[]{:S(2)}) copy-start(f32[16,1,128,256]{3,2,1,0:T(8,128)} %param.17) | copy-start | bytes 6291460
  0.0 4.9 %copy-start.3 = (bf16[16,1024]{1,0:T(8,128)(2,1)S(1)}, bf16[16,1024]{1,0:T(8,128)(2,1)}, u32[]{:S(2)}) copy-start(bf16[16,1024]{1,0:T(8,128)(2,1)} %param.15) | copy-start | bytes 98308
  0.0 4.9 %copy-start.8 = (f32[1024]{0:T(1024)S(1)}, f32[1024]{0:T(1024)}, u32[]{:S(2)}) copy-start(f32[1024]{0:T(1024)} %param.18) | copy-start | bytes 12292
  0.0 4.9 %copy-start.7 = (bf16[1024,256]{1,0:T(8,128)(2,1)S(1)}, bf16[1024,256]{1,0:T(8,128)(2,1)}, u32[]{:S(2)}) copy-start(bf16[1024,256]{1,0:T(8,128)(2,1)} %param.21) | copy-start | bytes 1572868
  0.0 5.4 %copy-start.2 = (bf16[256,1024]{1,0:T(8,128)(2,1)S(1)}, bf16[256,1024]{1,0:T(8,128)(2,1)}, u32[]{:S(2)}) copy-start(bf16[256,1024]{1,0:T(8,128)(2,1)} %param.23) | copy-start | bytes 1572868
  0.0 5.4 %copy-start.6 = (f32[256]{0:T(256)S(1)}, f32[256]{0:T(256)}, u32[]{:S(2)}) copy-start(f32[256]{0:T(256)} %param.22) | copy-start | bytes 3076
  3.1 8.1 %copy-start.4 = (f32[16,2]{0,1:T(2,128)S(1)}, f32[16,2]{0,1:T(2,128)}, u32[]{:S(2)}) copy-start(f32[16,2]{0,1:T(2,128)} %param.26) | copy-start | bytes 388
  3.1 8.2 %copy-start.5 = (s32[16,2]{0,1:T(2,128)S(1)}, s32[16,2]{0,1:T(2,128)}, u32[]{:S(2)}) copy-start(s32[16,2]{0,1:T(2,128)} %param.25) | copy-start | bytes 388
  6.4 9.7 %all-to-all-start = ((bf16[4,16,1024]{2,1,0:T(8,128)(2,1)}), bf16[4,16,1024]{2,1,0:T(8,128)(2,1)S(1)}, u32[]{:S(2)}, u32[]{:S(2)}) async-start(bf16[4,16,1024]{2,1,0:T(8,128)(2,1)} %broadcast_in_dim.4), calls=%async_computation | async-start | bytes 262144 | tf_op jit(solution)/shard_map/all_to_all | solution.py:27
  16.4 44.4 %copy-start.1 = (bf16[1,1024,448]{1,2,0:T(8,128)(2,1)S(1)}, bf16[1,1024,448]{1,2,0:T(8,128)(2,1)}, u32[]{:S(2)}) copy-start(bf16[1,1024,448]{1,2,0:T(8,128)(2,1)} %param.27) | copy-start | bytes 2752516
